TPU v7x, 32 devices: a whole 2x2x4 slice. The times are simulated.
32 devices in a mesh: ep: 4 (over y, x), tp: 8 (over z, core).
Axes of the slice: x: 2, y: 2, z: 4, core: 2. Of those that a mesh axis runs over, the one named last changes fastest.
Arguments:
- hidden: bfloat16 [160, 4096], P('ep', 'tp'), may hold values from -6 to 6
- positions: int32 [160], P('ep'), may hold values from 0 to 16383
- ret_state: float32 [160, 16, 128, 128], P('ep', 'tp'), may hold values from -1.5 to 1.5
- query_weight: bfloat16 [4096, 2048], P('ep', 'tp'), may hold values from -0.09375 to 0.09375
- key_weight: bfloat16 [4096, 2048], P('ep', 'tp'), may hold values from -0.09375 to 0.09375
- value_weight: bfloat16 [4096, 2048], P('ep', 'tp'), may hold values from -0.09375 to 0.09375
- gate_weight: bfloat16 [4096, 2048], P('ep', 'tp'), may hold values from -0.09375 to 0.09375
- head_gain: float32 [2048], P('tp'), may hold values from 0.1 to 1.9
- out_weight: bfloat16 [2048, 4096], P(None, 'tp'), may hold values from -0.125 to 0.125
- mix_gain: float32 [4096], replicated, may hold values from 0.1 to 1.9
- ffn_gain: float32 [4096], replicated, may hold values from 0.1 to 1.9
- expert_gate: bfloat16 [8, 4096, 2048], P('ep', None, 'tp'), may hold values from -0.09375 to 0.09375
- expert_up: bfloat16 [8, 4096, 2048], P('ep', None, 'tp'), may hold values from -0.09375 to 0.09375
- expert_down: bfloat16 [8, 2048, 4096], P('ep', None, 'tp'), may hold values from -0.125 to 0.125
- route_ids: int32 [160, 2], P('ep'), may hold values from 0 to 7, as said below
- route_weight: float32 [160, 2], P('ep'), may hold values from 0.25 to 1
Outputs:
- updated: bfloat16 [160, 4096], P('ep', 'tp')
- next_state: float32 [160, 16, 128, 128], P('ep', 'tp')
Inputs may be any that keep to these rules, and one draw needn't show every extreme that they name: `route_ids`: each row names two different experts of one group, the group being the numbers g * 2 to g * 2 + 1; in the rows of one device (aligned blocks of 40 rows) no expert is named more than 10 times, and some expert is named exactly 10 times.
All inputs are finite; a program needn't handle non-finite values.
Results may differ from a plain program's by a relative error of at most 0.014.
Values may be sent and summed in bfloat16 or wider, within the bound.
A program may use at most 64 MiB of HBM per device.

v0:
```python
import jax
import jax.numpy as jnp
from jax import lax
from jax.sharding import PartitionSpec as P

D = 4096
HEADS = 16
HEAD = 128
GROUPS = 4
TOP = 2


epsilon = 1e-06
rope_base = 10000.0


def rms_scale(rows, gain):
    values = rows.astype(jnp.float32)
    factor = lax.rsqrt(jnp.mean(values * values, axis=-1, keepdims=True) + epsilon)
    return (values * factor * gain).astype(jnp.bfloat16)


def log_decay(head_ids):
    return jnp.log(1.0 - 2.0 ** (-5.0 - 5.0 * head_ids.astype(jnp.float32) / (HEADS - 1)))


def rotate(values, positions):
    width = values.shape[-1]
    inverse = 1.0 / rope_base ** (jnp.arange(0, width, 2, dtype=jnp.float32) / width)
    angle = positions.astype(jnp.float32)[:, None, None] * inverse[None, None, :]
    cosine = jnp.cos(angle)
    sine = jnp.sin(angle)
    first = values[..., : width // 2]
    second = values[..., width // 2 :]
    return jnp.concatenate(
        [first * cosine - second * sine, first * sine + second * cosine], axis=-1
    )


def retain(query, key_rows, value_rows, gate_rows, ret_state, positions, head_ids, head_gain):
    batch = query.shape[0]
    heads = head_ids.shape[0]

    def split(array):
        return array.astype(jnp.float32).reshape(batch, heads, HEAD)

    rotated_query = rotate(split(query), positions)
    rotated_key = rotate(split(key_rows), positions) * HEAD ** (-0.5)
    value_heads = split(value_rows)
    decay = jnp.exp(log_decay(head_ids))
    next_state = (
        decay[None, :, None, None] * ret_state
        + rotated_key[..., :, None] * value_heads[..., None, :]
    )
    read = jnp.einsum("bhd,bhde->bhe", rotated_query, next_state, precision=lax.Precision.HIGHEST)
    centered = read - jnp.mean(read, axis=-1, keepdims=True)
    normal = centered * lax.rsqrt(jnp.mean(centered * centered, axis=-1, keepdims=True) + epsilon)
    mixed = (
        normal.reshape(batch, heads * HEAD) * head_gain * jax.nn.silu(gate_rows.astype(jnp.float32))
    )
    return (mixed.astype(jnp.bfloat16), next_state)


def per_device(
    hidden,
    positions,
    ret_state,
    query_weight,
    key_weight,
    value_weight,
    gate_weight,
    head_gain,
    out_weight,
    mix_gain,
    ffn_gain,
    expert_gate,
    expert_up,
    expert_down,
    route_ids,
    route_weight,
):
    own_rows = hidden.shape[0]
    slice_width = hidden.shape[1]
    full_rows = lax.all_gather(hidden, "tp", axis=1, tiled=True)
    normed = rms_scale(full_rows, mix_gain)
    columns = lax.all_to_all(normed, "ep", split_axis=1, concat_axis=0, tiled=True)
    stacked = jnp.concatenate([query_weight, key_weight, value_weight, gate_weight], axis=1)
    width = query_weight.shape[1]
    joined = lax.psum_scatter(
        jnp.dot(columns, stacked, preferred_element_type=jnp.float32),
        "ep",
        scatter_dimension=0,
        tiled=True,
    )
    sums = tuple((joined[:, number * width : (number + 1) * width] for number in range(4)))
    query, key_rows, value_rows, gate_rows = tuple((total.astype(jnp.bfloat16) for total in sums))
    heads_here = query_weight.shape[1] // HEAD
    head_ids = lax.axis_index("tp") * heads_here + jnp.arange(heads_here, dtype=jnp.int32)
    mixed, next_state = retain(
        query, key_rows, value_rows, gate_rows, ret_state, positions, head_ids, head_gain
    )
    projected = jnp.dot(
        lax.all_gather(mixed, "tp", axis=1, tiled=True),
        out_weight,
        preferred_element_type=jnp.float32,
    )
    after = (hidden.astype(jnp.float32) + projected).astype(jnp.bfloat16)
    local_experts = expert_gate.shape[0]
    peers = lax.axis_size("ep")
    experts = local_experts * peers
    group_size = experts // GROUPS
    capacity = 2 * ((own_rows // GROUPS + group_size - 1) // group_size)
    chosen = route_ids.reshape(-1)
    onehot = (chosen[:, None] == jnp.arange(experts, dtype=jnp.int32)[None, :]).astype(jnp.int32)
    ranks = jnp.sum((jnp.cumsum(onehot, axis=0) - 1) * onehot, axis=1)
    send_slot = chosen * capacity + ranks
    slot_count = experts * capacity
    placing = (jnp.arange(slot_count, dtype=jnp.int32)[:, None] == send_slot[None, :]).astype(
        jnp.float32
    )
    token_place = jnp.sum(placing.reshape(slot_count, own_rows, TOP), axis=2).astype(jnp.bfloat16)
    after_float = after.astype(jnp.float32)
    squares = lax.psum(jnp.sum(after_float * after_float, axis=1), "tp")
    gain_slice = lax.dynamic_slice_in_dim(
        ffn_gain, lax.axis_index("tp") * slice_width, slice_width, 0
    )
    factor = lax.rsqrt(squares / D + epsilon)
    scaled = (after_float * factor[:, None] * gain_slice).astype(jnp.bfloat16)
    packed = jnp.dot(token_place, scaled, preferred_element_type=jnp.float32).astype(jnp.bfloat16)
    arrived = lax.all_to_all(
        packed.reshape(peers, local_experts, capacity, scaled.shape[1]),
        "ep",
        split_axis=0,
        concat_axis=2,
        tiled=True,
    )
    arrived = lax.all_gather(arrived, "tp", axis=3, tiled=True)
    arrived = arrived.reshape(local_experts, peers * capacity, D)
    gate = jnp.einsum("emd,edf->emf", arrived, expert_gate, preferred_element_type=jnp.float32)
    lifted = jnp.einsum("emd,edf->emf", arrived, expert_up, preferred_element_type=jnp.float32)
    activated = (jax.nn.silu(gate) * lifted).astype(jnp.bfloat16)
    out_width = expert_down.shape[2]
    result = jnp.einsum(
        "emf,efd->emd",
        lax.all_gather(activated, "tp", axis=2, tiled=True),
        expert_down,
        preferred_element_type=jnp.float32,
    ).astype(jnp.bfloat16)
    back = lax.all_to_all(
        result.reshape(local_experts, peers, capacity, out_width),
        "ep",
        split_axis=1,
        concat_axis=1,
        tiled=True,
    )
    returned_rows = back.reshape(local_experts * peers * capacity, out_width)
    source_row = (
        chosen % local_experts * (peers * capacity) + chosen // local_experts * capacity + ranks
    )
    values = returned_rows[source_row].astype(jnp.float32).reshape(own_rows, TOP, out_width)
    weighted = jnp.sum(values * route_weight[:, :, None], axis=1)
    updated = (after.astype(jnp.float32) + weighted).astype(jnp.bfloat16)
    return (updated, next_state)


def solution(mesh):
    return jax.shard_map(
        per_device,
        mesh=mesh,
        in_specs=(
            P("ep", "tp"),
            P("ep"),
            P("ep", "tp", None, None),
            P("ep", "tp"),
            P("ep", "tp"),
            P("ep", "tp"),
            P("ep", "tp"),
            P("tp"),
            P(None, "tp"),
            P(),
            P(),
            P("ep", None, "tp"),
            P("ep", None, "tp"),
            P("ep", None, "tp"),
            P("ep", None),
            P("ep", None),
        ),
        out_specs=(P("ep", "tp"), P("ep", "tp", None, None)),
        check_vma=False,
    )
```

profile of v0, /device:TPU:0, one launch (start us, length us, event | category | flops | bytes accessed | tf_op | source)
XLA Modules:
  0.0 168.9 jit_solution(997779446454232462)
XLA Ops:
  7.2 16.4 %all_gather.12 = bf16[40,4096]{1,0:T(8,128)(2,1)S(1)} all-gather(bf16[40,512]{1,0:T(8,128)(2,1)} %param.16), channel_id=1, replica_groups=mesh['ep'=4,'tp'=8] {'tp'}, dimensions={1}, use_global_device_ids=true | all-gather | bytes 368640 | tf_op jit(solution)/shard_map/all_gather | solution.py:84
  23.8 0.9 fusion.13
  24.7 10.6 %all_to_all.42 = bf16[40,4,1024]{2,0,1:T(8,128)(2,1)S(1)} all-to-all(bf16[40,4,1024]{2,0,1:T(8,128)(2,1)S(1)} %bitcast.48), channel_id=1, replica_groups=mesh['ep'=4,'tp'=8] {'ep'}, dimensions={1} | all-to-all | bytes 655360 | tf_op jit(solution)/shard_map/all_to_all | solution.py:86
  35.3 2.9 %fusion = f32[160,1024]{1,0:T(8,128)} fusion(bf16[160,1024]{1,0:T(8,128)(2,1)S(1)} %bitcast.52, bf16[1024,256]{1,0:T(8,128)(2,1)} %param.22, bf16[1024,256]{1,0:T(8,128)(2,1)} %param.21, bf16[1024,256]{1,0:T(8,128)(2,1)} %param.20, bf16[1024,256]{1,0:T(8,128)(2,1)} %param.19), kind=kOutput, calls=%fused_computation.2 | convolution fusion | flops 343932928 | bytes 3080192 | tf_op jit(solution)/shard_map/dot_general | solution.py:90
  39.2 0.8 dynamic_slice.3
  40.3 23.2 %reduce-scatter.4.cloned.1.call-done = f32[40,1024]{1,0:T(8,128)} async-done(((f32[160,1024]{1,0:T(8,128)}), f32[40,1024]{1,0:T(8,128)}) %reduce-scatter.4.cloned.1.call-update) | async-done | bytes 163856
  63.4 0.9 convert.10
  64.9 4.0 %multiply_add_fusion = f32[40,2,128,128]{3,2,1,0:T(8,128)S(1)} fusion(f32[40,2,128,128]{3,2,1,0:T(8,128)} %param.18, f32[40,2,128]{2,1,0:T(2,128)S(1)} %reshape.305, f32[40,2,128]{2,1,0:T(2,128)S(1)} %get-tuple-element.16, f32[2]{0:T(128)S(1)} %log_exponential_fusion), kind=kLoop, calls=%fused_computation.1 | loop fusion | flops 3932160 | bytes 10567688 | tf_op jit(solution)/shard_map/add | solution.py:52
  68.9 2.3 %copy-done.1 = f32[40,2,128,128]{3,2,1,0:T(8,128)} copy-done((f32[40,2,128,128]{3,2,1,0:T(8,128)}, f32[40,2,128,128]{3,2,1,0:T(8,128)S(1)}, u32[]{:S(2)}) %copy-start.1) | copy-done | bytes 5242904
  71.3 4.5 %fusion.31 = f32[40,2,1,128]{3,2,1,0:T(1,128)S(1)} fusion(f32[40,2,128,1]{2,3,1,0:T(1,128)S(1)} %bitcast.55, f32[40,2,128,128]{3,2,1,0:T(8,128)S(1)} %multiply_add_fusion), kind=kOutput, calls=%fused_computation.78 | convolution fusion | flops 15728640 | bytes 5324800 | tf_op jit(solution)/shard_map/bhd,bhde->bhe/dot_general | solution.py:55
  76.4 14.2 %all_gather.13 = bf16[40,2048]{1,0:T(8,128)(2,1)S(1)} all-gather(bf16[40,256]{1,0:T(8,128)(2,1)S(1)} %fusion.24), channel_id=1, replica_groups=mesh['ep'=4,'tp'=8] {'tp'}, dimensions={1}, use_global_device_ids=true | all-gather | bytes 184320 | tf_op jit(solution)/shard_map/all_gather | solution.py:103
  91.1 16.8 %psum.7 = f32[40]{0:T(128)S(1)} all-reduce(f32[40]{0:T(128)S(1)} %get-tuple-element.13), channel_id=1, replica_groups=mesh['ep'=4,'tp'=8] {'tp'}, use_global_device_ids=true, to_apply=%region_8.9 | all-reduce | flops 40 | bytes 320 | tf_op jit(solution)/shard_map/psum | solution.py:123
  108.2 0.7 copy.67
  108.9 3.3 %all-to-all-start.1 = ((bf16[4,2,10,512]{3,1,2,0:T(2,128)(2,1)}), bf16[4,2,10,512]{3,1,2,0:T(2,128)(2,1)S(1)}, u32[]{:S(2)}, u32[]{:S(2)}) async-start(bf16[4,2,10,512]{3,1,2,0:T(2,128)(2,1)} %copy.67), calls=%async_computation.1 | async-start | bytes 163840 | tf_op jit(solution)/shard_map/all_to_all | solution.py:130
  112.3 4.7 %all-to-all-done.1 = bf16[4,2,10,512]{3,1,2,0:T(2,128)(2,1)S(1)} async-done(((bf16[4,2,10,512]{3,1,2,0:T(2,128)(2,1)}), bf16[4,2,10,512]{3,1,2,0:T(2,128)(2,1)S(1)}, u32[]{:S(2)}, u32[]{:S(2)}) %all-to-all-start.1) | async-done | bytes 81952 | tf_op jit(solution)/shard_map/all_to_all | solution.py:130
  117.0 15.5 %all_gather.14 = bf16[1,2,40,4096]{3,2,1,0:T(8,128)(2,1)S(1)} all-gather(bf16[1,2,40,512]{3,2,1,0:T(8,128)(2,1)S(1)} %copy.68), channel_id=1, replica_groups=mesh['ep'=4,'tp'=8] {'tp'}, dimensions={3}, use_global_device_ids=true | all-gather | bytes 737280 | tf_op jit(solution)/shard_map/all_gather | solution.py:137
  132.5 2.9 %fusion.15 = f32[2,40,256]{2,1,0:T(8,128)S(1)} fusion(bf16[2,4096,256]{2,1,0:T(8,128)(2,1)} %param.27, bf16[1,2,40,4096]{3,2,1,0:T(8,128)(2,1)S(1)} %all_gather.14), kind=kOutput, calls=%fused_computation.23 | convolution fusion | flops 167772160 | bytes 4931584 | tf_op jit(solution)/shard_map/emd,edf->emf/dot_general | solution.py:139
  135.4 0.7 fusion.8
  136.1 14.4 %all_gather.15 = bf16[2,40,2048]{2,1,0:T(8,128)(2,1)S(1)} all-gather(bf16[2,40,256]{2,1,0:T(8,128)(2,1)S(1)} %fusion.8), channel_id=1, replica_groups=mesh['ep'=4,'tp'=8] {'tp'}, dimensions={2}, use_global_device_ids=true | all-gather | bytes 368640 | tf_op jit(solution)/shard_map/all_gather | solution.py:145
  150.5 0.8 convolution_convert_fusion
  151.3 0.7 copy.69
  152.0 3.3 %all-to-all-start.2 = ((bf16[2,4,10,512]{3,0,2,1:T(2,128)(2,1)}), bf16[2,4,10,512]{3,0,2,1:T(2,128)(2,1)S(1)}, u32[]{:S(2)}, u32[]{:S(2)}) async-start(bf16[2,4,10,512]{3,0,2,1:T(2,128)(2,1)} %bitcast.10), calls=%async_computation.2 | async-start | bytes 163840 | tf_op jit(solution)/shard_map/all_to_all | solution.py:149
  155.4 4.8 %all-to-all-done.2 = bf16[2,4,10,512]{3,0,2,1:T(2,128)(2,1)S(1)} async-done(((bf16[2,4,10,512]{3,0,2,1:T(2,128)(2,1)}), bf16[2,4,10,512]{3,0,2,1:T(2,128)(2,1)S(1)}, u32[]{:S(2)}, u32[]{:S(2)}) %all-to-all-start.2) | async-done | bytes 81952 | tf_op jit(solution)/shard_map/all_to_all | solution.py:149
  160.3 0.7 gather_fusion
  (61 shorter events, 4.4 us)
Async XLA Ops:
  7.2 83.4 %copy-start = (bf16[2048,512]{1,0:T(8,128)(2,1)S(1)}, bf16[2048,512]{1,0:T(8,128)(2,1)}, u32[]{:S(2)}) copy-start(bf16[2048,512]{1,0:T(8,128)(2,1)} %param.24) | copy-start | bytes 6291460
  7.2 56.3 %reduce-scatter.4.cloned.1.call-start = ((), (), s32[]{:S(2)}) async-start(), calls=%async_computation.4 | async-start | bytes 819200
  35.3 2.9 %copy-start.5 = (s32[40,2]{0,1:T(2,128)S(1)}, s32[40,2]{0,1:T(2,128)}, u32[]{:S(2)}) copy-start(s32[40,2]{0,1:T(2,128)} %param.30) | copy-start | bytes 964
  35.3 3.3 %copy-start.8 = (s32[40]{0:T(128)S(1)}, s32[40]{0:T(128)}, u32[]{:S(2)}) copy-start(s32[40]{0:T(128)} %param.17) | copy-start | bytes 484
  68.9 2.4 %copy-start.1 = (f32[40,2,128,128]{3,2,1,0:T(8,128)}, f32[40,2,128,128]{3,2,1,0:T(8,128)S(1)}, u32[]{:S(2)}) copy-start(f32[40,2,128,128]{3,2,1,0:T(8,128)S(1)} %multiply_add_fusion) | copy-start | bytes 15728644
  68.9 7.4 %copy-start.7 = (f32[256]{0:T(256)S(1)}, f32[256]{0:T(256)}, u32[]{:S(2)}) copy-start(f32[256]{0:T(256)} %param.23) | copy-start | bytes 3076
  68.9 21.6 %copy-start.4 = (bf16[40,512]{1,0:T(8,128)(2,1)S(1)}, bf16[40,512]{1,0:T(8,128)(2,1)}, u32[]{:S(2)}) copy-start(bf16[40,512]{1,0:T(8,128)(2,1)} %param.16) | copy-start | bytes 122884
  71.3 40.9 %copy-start.6 = (f32[40,2]{0,1:T(2,128)S(1)}, f32[40,2]{0,1:T(2,128)}, u32[]{:S(2)}) copy-start(f32[40,2]{0,1:T(2,128)} %param.31) | copy-start | bytes 964
  108.9 8.2 %all-to-all-start.1 = ((bf16[4,2,10,512]{3,1,2,0:T(2,128)(2,1)}), bf16[4,2,10,512]{3,1,2,0:T(2,128)(2,1)S(1)}, u32[]{:S(2)}, u32[]{:S(2)}) async-start(bf16[4,2,10,512]{3,1,2,0:T(2,128)(2,1)} %copy.67), calls=%async_computation.1 | async-start | bytes 163840 | tf_op jit(solution)/shard_map/all_to_all | solution.py:130
  117.0 18.4 %copy-start.3 = (bf16[2,4096,256]{2,1,0:T(8,128)(2,1)S(1)}, bf16[2,4096,256]{2,1,0:T(8,128)(2,1)}, u32[]{:S(2)}) copy-start(bf16[2,4096,256]{2,1,0:T(8,128)(2,1)} %param.28) | copy-start | bytes 12582916
  135.4 15.1 %copy-start.2 = (bf16[2,2048,512]{2,1,0:T(8,128)(2,1)S(1)}, bf16[2,2048,512]{2,1,0:T(8,128)(2,1)}, u32[]{:S(2)}) copy-start(bf16[2,2048,512]{2,1,0:T(8,128)(2,1)} %param.29) | copy-start | bytes 12582916
  152.0 8.2 %all-to-all-start.2 = ((bf16[2,4,10,512]{3,0,2,1:T(2,128)(2,1)}), bf16[2,4,10,512]{3,0,2,1:T(2,128)(2,1)S(1)}, u32[]{:S(2)}, u32[]{:S(2)}) async-start(bf16[2,4,10,512]{3,0,2,1:T(2,128)(2,1)} %bitcast.10), calls=%async_computation.2 | async-start | bytes 163840 | tf_op jit(solution)/shard_map/all_to_all | solution.py:149
Sparse Core Ops, SparseCore 0:
  38.4 25.0 reduce-scatter.3
where the time goes:
time: 169 us
  blocking collectives  87.8 us (52%)
  waiting for transfers between devices  32.8 us (19%)
  between operations  14.4 us (9%)
  matrix products  12.6 us (7%)
  other arithmetic  8.45 us (5%)
  starting transfers between devices  6.62 us (4%)
  local copies, waits for them, and re-layouts  6.2 us (4%)
    unnamed x2, waiting for transfers between devices  23.2 us
    psum x1, blocking collectives, per_device(): squares = lax.psum(jnp.sum(after_float * after_float, axis=1), 'tp')  16.8 us
    all_gather x1, blocking collectives, per_device(): full_rows = lax.all_gather(hidden, 'tp', axis=1, tiled=True)  16.4 us
    all_gather x1, blocking collectives, per_device(): arrived = lax.all_gather(arrived, 'tp', axis=3, tiled=True)  15.5 us
    all_gather x1, blocking collectives, per_device(): lax.all_gather(activated, 'tp', axis=2, tiled=True)  14.4 us
    all_gather x1, blocking collectives, per_device(): lax.all_gather(mixed, 'tp', axis=1, tiled=True)  14.2 us
    all_to_all x1, blocking collectives, per_device(): lax.all_to_all(normed, 'ep', split_axis=1, concat_axis=0, tiled=True)  10.6 us
    all_to_all x1, waiting for transfers between devices, per_device(): lax.all_to_all(result.reshape(local_experts, peers, capacity, out_width),...  4.84 us
  transfers between devices with their start and end apart: 3, of which 3 were waited for; matrix products, arithmetic and copies ran while one was open for 1% of the time, Pallas kernels for 0%

commit v1 on v0

v1 whole, which is shorter than its diff:
```python
import functools

import jax
import jax.numpy as jnp
import numpy as np
from jax import lax
from jax.experimental import pallas as pl
from jax.experimental.pallas import tpu as pltpu
from jax.sharding import PartitionSpec as P

HEAD = 128
GROUPS = 4
TOP = 2
HEADS = 16
AUX = 128
epsilon = 1e-06
rope_base = 10000.0
MESH = pl.DeviceIdType.MESH
f32 = jnp.float32
bf16 = jnp.bfloat16


def thirds(x):
    hi = x.astype(bf16).astype(f32)
    mid = (x - hi).astype(bf16).astype(f32)
    return hi, mid, x - hi - mid


def dot(a, b):
    return jnp.dot(a, b, preferred_element_type=f32)


def kernel(c, hid, pos, inv, hgain, mgain, fgain, ids, rw, tab, perm, permt,
           wq, wk, wv, wg, wo_h, eg_h, eu_h, ed_h, st_h,
           out, nst_h,
           wqk, wo, wgu, wd, st, hg, nb, xb, pb, rb, qs, ks, vs, rd, ys, mg, xs, x1, ag, x2, acts, a2, yb, y1, y2,
           tsend, trecv, esend, erecv, lsem, osem):
    N, T, R, W, J, F = c.N, c.T, c.R, c.W, c.J, c.F
    Z = T // 2
    U, PU, SP, ME, cap = c.U, c.PU, c.SP, c.ME, c.cap
    heads, HW, D = c.heads, c.heads * HEAD, c.D
    e = lax.axis_index("ep")
    t = lax.axis_index("tp")
    z = t // 2
    core = t % 2
    sib = z * 2 + (1 - core)

    local = []

    def fetch(src, dst):
        cp = pltpu.make_async_copy(src, dst, lsem.at[len(local)])
        cp.start()
        local.append(cp)
        return cp

    proj_w = [fetch(w, wqk.at[:, pl.ds(n * HW, HW)]) for n, w in enumerate((wq, wk, wv, wg))]
    state_in = fetch(st_h, st)
    wo_in = fetch(wo_h, wo)
    gu_in = []
    for u in range(U):
        for i in range(PU):
            gu_in.append(fetch(eg_h.at[u * PU + i], wgu.at[u, :, pl.ds(2 * i * F, F)]))
            gu_in.append(fetch(eu_h.at[u * PU + i], wgu.at[u, :, pl.ds((2 * i + 1) * F, F)]))
    wd_in = fetch(ed_h, wd)

    barrier = pltpu.get_barrier_semaphore()
    for i in range(1, N):
        pl.semaphore_signal(barrier, inc=1, device_id=(lax.rem(e + i, N), t), device_id_type=MESH)
    for i in range(1, Z):
        pl.semaphore_signal(barrier, inc=1, device_id=(e, lax.rem(z + i, Z) * 2 + core), device_id_type=MESH)
    pl.semaphore_signal(barrier, inc=1, device_id=(e, sib), device_id_type=MESH)

    angle = pos[...].astype(f32) * inv[...]
    cosine = jnp.cos(angle)
    lane = lax.broadcasted_iota(jnp.int32, (R, HEAD), 1)
    sine = jnp.where(lane < HEAD // 2, -1.0, 1.0) * jnp.sin(angle)

    S = N * SP
    base = tab[0:1, :]
    want = tab[1:2, :]
    masks = [
        jnp.where((ids[:, k : k + 1] >= base) & (ids[:, k : k + 1] < base + PU), 1.0, 0.0) for k in range(TOP)
    ]
    member = functools.reduce(jnp.maximum, masks)
    row = lax.broadcasted_iota(jnp.int32, (R, R), 0)
    col = lax.broadcasted_iota(jnp.int32, (R, R), 1)
    lower = jnp.where(col < row, 1.0, 0.0).astype(bf16)
    rank = dot(lower, member.astype(bf16))
    hit = jnp.where(rank == want.astype(f32), 1.0, 0.0)
    place = member * hit
    place_t = jnp.transpose(place).astype(bf16)
    places_t = [jnp.transpose(m * hit).astype(bf16) for m in masks]
    lane_a = lax.broadcasted_iota(jnp.int32, (R, AUX), 1)
    aux_w = jnp.zeros((S, AUX), f32)
    for k in range(TOP):
        parts = thirds(rw[:, k : k + 1])
        which = (ids[:, k : k + 1] & (PU - 1)) * 3 + 3
        lanes = jnp.zeros((R, AUX), f32)
        for n in range(3):
            lanes = lanes + jnp.where(lane_a == which + n, parts[n], 0.0)
        aux_w = aux_w + dot(places_t[k], lanes.astype(bf16))

    pl.semaphore_wait(barrier, N - 1 + Z - 1 + 1)

    def tp_gather(ph, src, buf, use):
        sends = []

        def send(s, slot, peer, n):
            cp = pltpu.make_async_remote_copy(
                src_ref=s, dst_ref=buf.at[slot], send_sem=tsend.at[ph, n], recv_sem=trecv.at[ph, slot],
                device_id=(e, peer), device_id_type=MESH)
            cp.start()
            sends.append(cp)

        def arrive(slot, peer):
            pltpu.make_async_remote_copy(
                src_ref=src, dst_ref=buf.at[slot], send_sem=tsend.at[ph, 0], recv_sem=trecv.at[ph, slot],
                device_id=(e, peer), device_id_type=MESH).wait_recv()

        order = sorted(range(1, Z), key=lambda i: (min(i, Z - i), i))
        far = [lax.rem(z + i, Z) for i in order]
        for n, zz in enumerate(far):
            send(src, t, zz * 2 + core, n)
        send(src, t, sib, Z - 1)
        use(t, src)
        for n, zz in enumerate(far):
            slot = zz * 2 + core
            arrive(slot, slot)
            send(buf.at[slot], slot, sib, Z + n)
            if n == 0:
                arrive(sib, sib)
                use(sib, buf.at[sib])
            use(slot, buf.at[slot])
        for n, zz in enumerate(far):
            slot = zz * 2 + (1 - core)
            arrive(slot, sib)
            use(slot, buf.at[slot])
        return sends

    def ep_send(ph, i, src, buf):
        cp = pltpu.make_async_remote_copy(
            src_ref=src, dst_ref=buf.at[e], send_sem=esend.at[ph, i], recv_sem=erecv.at[ph, e],
            device_id=(lax.rem(e + i, N), t), device_id_type=MESH)
        cp.start()
        return cp

    def ep_arrive(ph, i, buf):
        peer = lax.rem(e + i, N)
        pltpu.make_async_remote_copy(
            src_ref=buf.at[peer], dst_ref=buf.at[peer], send_sem=esend.at[ph, i], recv_sem=erecv.at[ph, peer],
            device_id=(peer, t), device_id_type=MESH).wait_recv()

    done = []

    hbox = [jnp.zeros((R, W), f32)]

    def square(slot, ref):
        v = ref[...].astype(f32)
        hbox[0] = hbox[0] + v * v

    done += tp_gather(0, hid, hg, square)
    hg[t] = hid[...]
    factor = lax.rsqrt(jnp.sum(hbox[0], axis=1, keepdims=True) / D + epsilon)

    def norm_block(slot):
        g = mgain[:, pl.ds(pl.multiple_of(slot * W, W), W)]
        return (hg[slot].astype(f32) * factor * g).astype(bf16)

    for i in range(1, N):
        peer = lax.rem(e + i, N)
        for j in range(J):
            nb[peer, j] = norm_block(peer * J + j)
        done.append(ep_send(0, i, nb.at[peer], xb))
    for j in range(J):
        nb[e, j] = norm_block(e * J + j)

    for cp in proj_w:
        cp.wait()

    def project(ref, slot):
        return sum(dot(ref[slot, j], wqk[j * W : (j + 1) * W, :]) for j in range(J))

    total = project(nb, e)
    for i in range(1, N):
        ep_arrive(0, i, xb)
        peer = lax.rem(e + i, N)
        pb[peer] = project(xb, peer).astype(bf16)
        done.append(ep_send(1, i, pb.at[peer], rb))
    for i in range(1, N):
        ep_arrive(1, i, rb)
        total = total + rb[lax.rem(e + i, N)].astype(f32)
    total = total.astype(bf16).astype(f32)

    vs[...] = total[:, 2 * HW : 3 * HW]
    for h in range(heads):
        at = slice(h * HEAD, (h + 1) * HEAD)
        q = total[:, h * HEAD : (h + 1) * HEAD]
        k = total[:, HW + h * HEAD : HW + (h + 1) * HEAD]
        qs[:, at] = q * cosine + pltpu.roll(q, HEAD // 2, 1) * sine
        ks[:, at] = (k * cosine + pltpu.roll(k, HEAD // 2, 1) * sine) * HEAD ** (-0.5)
    decays = []
    for h in range(heads):
        number = (jnp.zeros((1, HEAD), jnp.int32) + (t * heads + h)).astype(f32)
        decays.append(1.0 - jnp.exp2(-5.0 - 5.0 * number / (HEADS - 1)))
    state_in.wait()

    def group(g, carry):
        rows = pl.ds(pl.multiple_of(g * 8, 8), 8)
        for h in range(heads):
            at = slice(h * HEAD, (h + 1) * HEAD)
            qt = jnp.transpose(qs[rows, at])
            kt = jnp.transpose(ks[rows, at])
            v8 = vs[rows, at]
            reads = []
            for b in range(8):
                new = decays[h] * st[g * 8 + b, h] + kt[:, b : b + 1] * v8[b : b + 1, :]
                st[g * 8 + b, h] = new
                reads.append(jnp.sum(qt[:, b : b + 1] * new, axis=0, keepdims=True))
            rd[rows, at] = jnp.concatenate(reads, axis=0)
        return carry

    lax.fori_loop(0, R // 8, group, 0)
    state_out = pltpu.make_async_copy(st, nst_h, osem)
    state_out.start()

    for h in range(heads):
        at = slice(h * HEAD, (h + 1) * HEAD)
        read = rd[:, at]
        centered = read - jnp.mean(read, axis=1, keepdims=True)
        normal = centered * lax.rsqrt(jnp.mean(centered * centered, axis=1, keepdims=True) + epsilon)
        gate = total[:, 3 * HW + h * HEAD : 3 * HW + (h + 1) * HEAD]
        ys[:, at] = (normal * hgain[:, at] * (gate * jax.nn.sigmoid(gate))).astype(bf16)

    wo_in.wait()
    pbox = [jnp.zeros((R, W), f32)]

    def out_project(slot, ref):
        w = wo[pl.ds(pl.multiple_of(slot * HW, HW), HW), :]
        pbox[0] = pbox[0] + dot(ref[...], w)

    done += tp_gather(1, ys, mg, out_project)
    after = (hid[...].astype(f32) + pbox[0]).astype(bf16).astype(f32)

    squares = thirds(jnp.sum(after * after, axis=1, keepdims=True))
    lanes = jnp.zeros((R, AUX), f32)
    for n in range(3):
        lanes = lanes + jnp.where(lane_a == n, squares[n], 0.0)
    gained = (after * fgain[:, pl.ds(pl.multiple_of(t * W, W), W)]).astype(bf16)
    packed = dot(place_t, gained).astype(bf16)
    packed_aux = (dot(place_t, lanes.astype(bf16)) + aux_w).astype(bf16)
    for n in range(N):
        xs[n, :, 0:W] = packed[n * SP : (n + 1) * SP, :]
        xs[n, :, W:] = packed_aux[n * SP : (n + 1) * SP, :]
    for i in range(1, N):
        done.append(ep_send(2, i, xs.at[lax.rem(e + i, N)], x1))
    x1[e] = xs[e]
    for i in range(1, N):
        ep_arrive(2, i, x1)
    own = dot(perm[...], x1[...].reshape(S, W + AUX)).astype(bf16)
    ag[...] = own
    weight_aux = own[:, W:].astype(f32)
    for cp in gu_in:
        cp.wait()
    MU = ME // U
    fbox = [jnp.zeros((ME, AUX), f32)] + [jnp.zeros((MU, PU * 2 * F), f32) for u in range(U)]

    def first(slot, ref):
        fbox[0] = fbox[0] + ref[:, W:].astype(f32)
        at = pl.ds(pl.multiple_of(slot * W, W), W)
        for u in range(U):
            fbox[1 + u] = fbox[1 + u] + dot(ref[u * MU : (u + 1) * MU, 0:W], wgu[u, at, :])

    done += tp_gather(2, ag, x2, first)
    sq = fbox[0][:, 0:1] + fbox[0][:, 1:2] + fbox[0][:, 2:3]
    scale = lax.rsqrt(sq / D + epsilon)
    for u in range(U):
        both = fbox[1 + u] * scale[u * MU : (u + 1) * MU, :]
        for i in range(PU):
            gate = both[:, 2 * i * F : (2 * i + 1) * F]
            lifted = both[:, (2 * i + 1) * F : (2 * i + 2) * F]
            acts[u * MU : (u + 1) * MU, i * F : (i + 1) * F] = (gate * jax.nn.sigmoid(gate) * lifted).astype(bf16)

    wd_in.wait()
    dbox = [jnp.zeros((MU, W), f32) for _ in range(U * PU)]

    def second(slot, ref):
        at = pl.ds(pl.multiple_of(slot * F, F), F)
        for u in range(U):
            for i in range(PU):
                n = u * PU + i
                dbox[n] = dbox[n] + dot(ref[u * MU : (u + 1) * MU, i * F : (i + 1) * F], wd[n, at, :])

    done += tp_gather(3, acts, a2, second)
    for u in range(U):
        mixture = jnp.zeros((MU, W), f32)
        for i in range(PU):
            three = weight_aux[u * MU : (u + 1) * MU, 3 + 3 * i : 6 + 3 * i]
            mixture = mixture + dbox[u * PU + i] * (three[:, 0:1] + three[:, 1:2] + three[:, 2:3])
        yb[u * MU : (u + 1) * MU, :] = mixture.astype(bf16)
    y1[...] = dot(permt[...], yb[...]).astype(bf16).reshape(N, SP, W)
    for i in range(1, N):
        done.append(ep_send(3, i, y1.at[lax.rem(e + i, N)], y2))
    y2[e] = y1[e]
    for i in range(1, N):
        ep_arrive(3, i, y2)
    out[...] = (after + dot(place.astype(bf16), y2[...].reshape(S, W))).astype(bf16)

    for cp in done:
        cp.wait_send()
    state_out.wait()


class Sizes:
    pass


def per_device(hidden, positions, ret_state, query_weight, key_weight, value_weight, gate_weight, head_gain,
               out_weight, mix_gain, ffn_gain, expert_gate, expert_up, expert_down, route_ids, route_weight):
    c = Sizes()
    c.N = N = lax.axis_size("ep")
    c.T = T = lax.axis_size("tp")
    c.R, c.W = R, W = hidden.shape
    c.D = D = mix_gain.shape[0]
    c.J = J = query_weight.shape[0] // W
    c.F = F = expert_gate.shape[2]
    c.heads = heads = query_weight.shape[1] // HEAD
    HW = heads * HEAD
    local_experts = expert_gate.shape[0]
    group_size = local_experts * N // GROUPS
    c.cap = cap = 2 * ((R // GROUPS + group_size - 1) // group_size)
    c.PU = PU = TOP if group_size == TOP and local_experts % TOP == 0 else 1
    c.U = U = local_experts // PU
    c.SP = SP = (U * cap + 15) // 16 * 16
    c.ME = ME = U * N * cap
    S = N * SP
    assert J * W * N == D and T % 2 == 0 and R % 8 == 0

    tab = np.full((2, S), -1000, np.int32)
    perm = np.zeros((ME, S), np.float32)
    for n in range(N):
        for u in range(U):
            for r in range(cap):
                s = n * SP + u * cap + r
                tab[0, s] = (n * U + u) * PU
                tab[1, s] = r
                perm[(u * N + n) * cap + r, s] = 1.0
    half = np.arange(0, HEAD, 2, dtype=np.float32) / HEAD
    inv = (1.0 / rope_base ** half.astype(np.float64)).astype(np.float32)
    inv = np.concatenate([inv, inv])[None, :]

    V = pl.BlockSpec(memory_space=pltpu.VMEM)
    A = pl.BlockSpec(memory_space=pl.ANY)
    names = [
        ((D // N, 4 * HW), bf16),
        ((T * HW, W), bf16),
        ((U, D, PU * 2 * F), bf16),
        (expert_down.shape, bf16),
        (ret_state.shape, f32),
        ((T, R, W), bf16),
        ((N, J, R, W), bf16),
        ((N, J, R, W), bf16),
        ((N, R, 4 * HW), bf16),
        ((N, R, 4 * HW), bf16),
        ((R, HW), f32),
        ((R, HW), f32),
        ((R, HW), f32),
        ((R, HW), f32),
        ((R, HW), bf16),
        ((T, R, HW), bf16),
        ((N, SP, W + AUX), bf16),
        ((N, SP, W + AUX), bf16),
        ((ME, W + AUX), bf16),
        ((T, ME, W + AUX), bf16),
        ((ME, PU * F), bf16),
        ((T, ME, PU * F), bf16),
        ((ME, W), bf16),
        ((N, SP, W), bf16),
        ((N, SP, W), bf16),
    ]
    updated, next_state = pl.pallas_call(
        functools.partial(kernel, c),
        out_shape=(jax.ShapeDtypeStruct((R, W), bf16), jax.ShapeDtypeStruct(ret_state.shape, f32)),
        in_specs=[V] * 11 + [A] * 9,
        out_specs=(V, A),
        scratch_shapes=[pltpu.VMEM(shape, kind) for shape, kind in names] + [
            pltpu.SemaphoreType.DMA((4, T)),
            pltpu.SemaphoreType.DMA((4, T)),
            pltpu.SemaphoreType.DMA((4, N)),
            pltpu.SemaphoreType.DMA((4, N)),
            pltpu.SemaphoreType.DMA((7 + 2 * local_experts,)),
            pltpu.SemaphoreType.DMA,
        ],
        compiler_params=pltpu.CompilerParams(
            collective_id=0, has_side_effects=True, vmem_limit_bytes=48 * 1024 * 1024
        ),
    )(hidden, positions.reshape(R, 1), jnp.asarray(inv), head_gain.reshape(1, HW), mix_gain.reshape(1, D),
      ffn_gain.reshape(1, D), route_ids, route_weight, jnp.asarray(tab), jnp.asarray(perm, bf16),
      jnp.asarray(perm.T, bf16),
      query_weight, key_weight, value_weight, gate_weight, out_weight, expert_gate, expert_up, expert_down, ret_state)
    return updated, next_state


def solution(mesh):
    return jax.shard_map(
        per_device,
        mesh=mesh,
        in_specs=(
            P("ep", "tp"), P("ep"), P("ep", "tp", None, None),
            P("ep", "tp"), P("ep", "tp"), P("ep", "tp"), P("ep", "tp"),
            P("tp"), P(None, "tp"), P(), P(),
            P("ep", None, "tp"), P("ep", None, "tp"), P("ep", None, "tp"),
            P("ep", None), P("ep", None),
        ),
        out_specs=(P("ep", "tp"), P("ep", "tp", None, None)),
        check_vma=False,
    )
```

time: 169 us -> 75.7 us (0.45)
  blocking collectives: 87.8 us -> 0 us
  Pallas kernels: 0 us -> 54.6 us
  waiting for transfers between devices: 32.8 us -> 0 us
  between operations: 14.4 us -> 0.65 us
  local copies, waits for them, and re-layouts: 6.2 us -> 19.8 us
  matrix products: 12.6 us -> 0 us
  other arithmetic: 8.45 us -> 0 us
  starting transfers between devices: 6.62 us -> 0 us
    all_gather x4 -> x0, blocking collectives: 60.5 us -> none  [the longest x1 16.4 us: per_device(): full_rows = lax.all_gather(hidden, 'tp', axis=1, tiled=True)]
    pallas_call x0 -> x1, Pallas kernels: none -> 54.6 us  [per_device(): pl.pallas_call(functools.partial(kernel, c), out_shape=(jax.ShapeDtypeStr...]
    unnamed x2 -> x0, waiting for transfers between devices: 23.2 us -> none
    psum x1 -> x0, blocking collectives: 16.8 us -> none  [per_device(): squares = lax.psum(jnp.sum(after_float * after_float, axis=1), 'tp')]
    unnamed x20 -> x30, local copies, waits for them, and re-layouts: 2.56 us -> 19 us
    dot_general x7 -> x0, matrix products: 12.6 us -> none  [the longest x1 4.55 us: retain(): jnp.einsum('bhd,bhde->bhe', rotated_query, next_state, precision=lax.Prec...]
    all_to_all x1 -> x0, blocking collectives: 10.6 us -> none  [per_device(): lax.all_to_all(normed, 'ep', split_axis=1, concat_axis=0, tiled=True)]
    all_to_all x2 -> x0, waiting for transfers between devices: 9.58 us -> none  [the longest x1 4.84 us: per_device(): lax.all_to_all(result.reshape(local_experts, peers, capacity, out_width),...]
  transfers between devices with their start and end apart: 3 -> 0, of which waited for: 3 -> 0; matrix products, arithmetic and copies ran while one was open for 1% -> 0% of each run, Pallas kernels for 0% -> 0%
where the time goes in v1:
time: 75.7 us; the launch traced here: 75 us
  Pallas kernels  54.6 us (72%)
  local copies, waits for them, and re-layouts  19.8 us (26%)
    pallas_call x1, Pallas kernels, per_device(): pl.pallas_call(functools.partial(kernel, c), out_shape=(jax.ShapeDtypeStr...  54.6 us
    unnamed x30, local copies, waits for them, and re-layouts  19 us

profile of v1, /device:TPU:0, one launch (start us, length us, event | category | flops | bytes accessed | tf_op | source)
XLA Modules:
  0.0 75.0 jit_solution(17388738325225444796)
XLA Ops:
  0.6 0.7 copy.22.pos
  1.4 0.8 %copy.23.ids = s32[40,2]{1,0:T(8,128)S(1)} copy(s32[40,2]{0,1:T(2,128)} %param.34) | data formatting | bytes 640 | tf_op args[14]
  2.1 0.8 %copy.24.rw = f32[40,2]{1,0:T(8,128)S(1)} copy(f32[40,2]{0,1:T(2,128)} %param.35) | data formatting | bytes 640 | tf_op args[15]
  2.9 0.0 copy-start
  2.9 1.6 %copy-done = bf16[2048,512]{1,0:T(8,128)(2,1)S(1)} copy-done((bf16[2048,512]{1,0:T(8,128)(2,1)S(1)}, bf16[2048,512]{1,0:T(8,128)(2,1)}, u32[]{:S(2)}) %copy-start) | copy-done | bytes 2097176
  4.5 0.0 copy-start.1
  4.5 1.0 %copy-done.1 = bf16[1024,256]{1,0:T(8,128)(2,1)S(1)} copy-done((bf16[1024,256]{1,0:T(8,128)(2,1)S(1)}, bf16[1024,256]{1,0:T(8,128)(2,1)}, u32[]{:S(2)}) %copy-start.1) | copy-done | bytes 524312
  5.5 0.0 copy-start.2
  5.5 1.0 %copy-done.2 = bf16[1024,256]{1,0:T(8,128)(2,1)S(1)} copy-done((bf16[1024,256]{1,0:T(8,128)(2,1)S(1)}, bf16[1024,256]{1,0:T(8,128)(2,1)}, u32[]{:S(2)}) %copy-start.2) | copy-done | bytes 524312
  6.6 0.0 copy-start.3
  6.6 1.0 %copy-done.3 = bf16[1024,256]{1,0:T(8,128)(2,1)S(1)} copy-done((bf16[1024,256]{1,0:T(8,128)(2,1)S(1)}, bf16[1024,256]{1,0:T(8,128)(2,1)}, u32[]{:S(2)}) %copy-start.3) | copy-done | bytes 524312
  7.6 1.0 %copy-done.4 = bf16[1024,256]{1,0:T(8,128)(2,1)S(1)} copy-done((bf16[1024,256]{1,0:T(8,128)(2,1)S(1)}, bf16[1024,256]{1,0:T(8,128)(2,1)}, u32[]{:S(2)}) %copy-start.4) | copy-done | bytes 524312
  8.7 0.0 copy-start.5
  8.7 0.8 %copy-done.5 = bf16[40,512]{1,0:T(8,128)(2,1)S(1)} copy-done((bf16[40,512]{1,0:T(8,128)(2,1)S(1)}, bf16[40,512]{1,0:T(8,128)(2,1)}, u32[]{:S(2)}) %copy-start.5) | copy-done | bytes 40984
  9.4 0.7 copy-done.6
  10.2 0.7 copy-done.7
  10.9 0.7 copy-done.8
  11.6 0.7 copy-done.9
  12.3 0.7 copy-done.10
  13.0 0.7 copy-done.11
  13.6 0.7 copy-done.12
  14.3 54.6 %shard_map.203 = (bf16[40,512]{1,0:T(8,128)(2,1)S(1)}, f32[40,2,128,128]{3,2,1,0:T(8,128)}) custom-call(bf16[40,512]{1,0:T(8,128)(2,1)S(1)} %copy-done.5, s32[40,1]{1,0:T(8,128)S(1)} %copy.22.pos, f32[1,128]{1,0:T(1,128)S(1)} %copy-done.12, f32[1,256]{1,0:T(1,128)S(1)} %bitcast.6, f32[1,4096]{1,0:T(1,128)S(1)} %bitcast.4, f32[1,4096]{1,0:T(1,128)S(1)} %bitcast.5, ...), custom_call_target="tpu_custom_call" | custom-call | tf_op jit(solution)/shard_map/pallas_call | solution.py:380
  68.9 0.6 copy.27
  69.5 5.5 %copy.28 = f32[40,2,128,128]{3,2,1,0:T(8,128)} copy(f32[40,2,128,128]{3,2,1,0:T(8,128)} %get-tuple-element.5) | data formatting | bytes 10485760
  (8 shorter events, 0.0 us)
Async XLA Ops:
  2.9 1.6 %copy-start = (bf16[2048,512]{1,0:T(8,128)(2,1)S(1)}, bf16[2048,512]{1,0:T(8,128)(2,1)}, u32[]{:S(2)}) copy-start(bf16[2048,512]{1,0:T(8,128)(2,1)} %wo_h.1) | copy-start | bytes 6291460
  4.5 1.0 %copy-start.1 = (bf16[1024,256]{1,0:T(8,128)(2,1)S(1)}, bf16[1024,256]{1,0:T(8,128)(2,1)}, u32[]{:S(2)}) copy-start(bf16[1024,256]{1,0:T(8,128)(2,1)} %wq.1) | copy-start | bytes 1572868
  5.5 1.0 %copy-start.2 = (bf16[1024,256]{1,0:T(8,128)(2,1)S(1)}, bf16[1024,256]{1,0:T(8,128)(2,1)}, u32[]{:S(2)}) copy-start(bf16[1024,256]{1,0:T(8,128)(2,1)} %wk.1) | copy-start | bytes 1572868
  6.6 1.0 %copy-start.3 = (bf16[1024,256]{1,0:T(8,128)(2,1)S(1)}, bf16[1024,256]{1,0:T(8,128)(2,1)}, u32[]{:S(2)}) copy-start(bf16[1024,256]{1,0:T(8,128)(2,1)} %wv.1) | copy-start | bytes 1572868
  7.6 1.0 %copy-start.4 = (bf16[1024,256]{1,0:T(8,128)(2,1)S(1)}, bf16[1024,256]{1,0:T(8,128)(2,1)}, u32[]{:S(2)}) copy-start(bf16[1024,256]{1,0:T(8,128)(2,1)} %wg.1) | copy-start | bytes 1572868
  8.7 0.8 %copy-start.5 = (bf16[40,512]{1,0:T(8,128)(2,1)S(1)}, bf16[40,512]{1,0:T(8,128)(2,1)}, u32[]{:S(2)}) copy-start(bf16[40,512]{1,0:T(8,128)(2,1)} %hid.1) | copy-start | bytes 122884
  9.4 0.7 copy-start.6
  10.1 0.7 copy-start.7
  10.9 0.7 copy-start.8
  11.6 0.7 copy-start.9
  12.3 0.7 copy-start.10
  13.0 0.7 copy-start.11
  13.6 0.7 copy-start.12

commit v2 on v1

--- a/solution.py
+++ b/solution.py
@@ -30,11 +30,12 @@
     return jnp.dot(a, b, preferred_element_type=f32)
 
 
-def kernel(c, hid, pos, inv, hgain, mgain, fgain, ids, rw, tab, perm, permt,
+def kernel(c, hid_h, pos_h, inv_h, hgain_h, mgain_h, fgain_h, ids_h, rw_h, tab_h, perm_h, permt_h,
            wq, wk, wv, wg, wo_h, eg_h, eu_h, ed_h, st_h,
-           out, nst_h,
-           wqk, wo, wgu, wd, st, hg, nb, xb, pb, rb, qs, ks, vs, rd, ys, mg, xs, x1, ag, x2, acts, a2, yb, y1, y2,
-           tsend, trecv, esend, erecv, lsem, osem):
+           out, st,
+           hid, pos, inv, hgain, mgain, fgain, idr, rwr, tab, perm, permt,
+           wqk, wo, wgu, wd, hg, nb, xb, pb, rb, qs, ks, vs, rd, ys, mg, xs, x1, ag, x2, acts, a2, yb, y1, y2,
+           tsend, trecv, esend, erecv, lsem):
     N, T, R, W, J, F = c.N, c.T, c.R, c.W, c.J, c.F
     Z = T // 2
     U, PU, SP, ME, cap = c.U, c.PU, c.SP, c.ME, c.cap
@@ -53,6 +54,10 @@
         local.append(cp)
         return cp
 
+    hid_in = fetch(hid_h, hid)
+    small = [fetch(a, b) for a, b in (
+        (pos_h, pos), (inv_h, inv), (hgain_h, hgain), (mgain_h, mgain), (fgain_h, fgain), (ids_h, idr), (rw_h, rwr),
+        (tab_h, tab), (perm_h, perm), (permt_h, permt))]
     proj_w = [fetch(w, wqk.at[:, pl.ds(n * HW, HW)]) for n, w in enumerate((wq, wk, wv, wg))]
     state_in = fetch(st_h, st)
     wo_in = fetch(wo_h, wo)
@@ -70,7 +75,17 @@
         pl.semaphore_signal(barrier, inc=1, device_id=(e, lax.rem(z + i, Z) * 2 + core), device_id_type=MESH)
     pl.semaphore_signal(barrier, inc=1, device_id=(e, sib), device_id_type=MESH)
 
-    angle = pos[...].astype(f32) * inv[...]
+    for cp in small:
+        cp.wait()
+    row = lax.broadcasted_iota(jnp.int32, (R, R), 0)
+    col = lax.broadcasted_iota(jnp.int32, (R, R), 1)
+
+    def stand(line):
+        return jnp.sum(jnp.where(row == col, line, 0.0), axis=1, keepdims=True)
+
+    ids = [stand(idr[k : k + 1, :].astype(f32)).astype(jnp.int32) for k in range(TOP)]
+    rw = [stand(rwr[k : k + 1, :]) for k in range(TOP)]
+    angle = stand(pos[...].astype(f32)) * inv[...]
     cosine = jnp.cos(angle)
     lane = lax.broadcasted_iota(jnp.int32, (R, HEAD), 1)
     sine = jnp.where(lane < HEAD // 2, -1.0, 1.0) * jnp.sin(angle)
@@ -79,11 +94,9 @@
     base = tab[0:1, :]
     want = tab[1:2, :]
     masks = [
-        jnp.where((ids[:, k : k + 1] >= base) & (ids[:, k : k + 1] < base + PU), 1.0, 0.0) for k in range(TOP)
+        jnp.where((ids[k] >= base) & (ids[k] < base + PU), 1.0, 0.0) for k in range(TOP)
     ]
     member = functools.reduce(jnp.maximum, masks)
-    row = lax.broadcasted_iota(jnp.int32, (R, R), 0)
-    col = lax.broadcasted_iota(jnp.int32, (R, R), 1)
     lower = jnp.where(col < row, 1.0, 0.0).astype(bf16)
     rank = dot(lower, member.astype(bf16))
     hit = jnp.where(rank == want.astype(f32), 1.0, 0.0)
@@ -93,13 +106,14 @@
     lane_a = lax.broadcasted_iota(jnp.int32, (R, AUX), 1)
     aux_w = jnp.zeros((S, AUX), f32)
     for k in range(TOP):
-        parts = thirds(rw[:, k : k + 1])
-        which = (ids[:, k : k + 1] & (PU - 1)) * 3 + 3
+        parts = thirds(rw[k])
+        which = (ids[k] & (PU - 1)) * 3 + 3
         lanes = jnp.zeros((R, AUX), f32)
         for n in range(3):
             lanes = lanes + jnp.where(lane_a == which + n, parts[n], 0.0)
         aux_w = aux_w + dot(places_t[k], lanes.astype(bf16))
 
+    hid_in.wait()
     pl.semaphore_wait(barrier, N - 1 + Z - 1 + 1)
 
     def tp_gather(ph, src, buf, use):
@@ -220,8 +234,6 @@
         return carry
 
     lax.fori_loop(0, R // 8, group, 0)
-    state_out = pltpu.make_async_copy(st, nst_h, osem)
-    state_out.start()
 
     for h in range(heads):
         at = slice(h * HEAD, (h + 1) * HEAD)
@@ -307,7 +319,6 @@
 
     for cp in done:
         cp.wait_send()
-    state_out.wait()
 
 
 class Sizes:
@@ -349,13 +360,23 @@
     inv = np.concatenate([inv, inv])[None, :]
 
     V = pl.BlockSpec(memory_space=pltpu.VMEM)
-    A = pl.BlockSpec(memory_space=pl.ANY)
+    A = pl.BlockSpec(memory_space=pltpu.HBM)
     names = [
+        ((R, W), bf16),
+        ((1, R), jnp.int32),
+        ((1, HEAD), f32),
+        ((1, HW), f32),
+        ((1, D), f32),
+        ((1, D), f32),
+        ((TOP, R), jnp.int32),
+        ((TOP, R), f32),
+        ((2, S), jnp.int32),
+        ((ME, S), bf16),
+        ((S, ME), bf16),
         ((D // N, 4 * HW), bf16),
         ((T * HW, W), bf16),
         ((U, D, PU * 2 * F), bf16),
         (expert_down.shape, bf16),
-        (ret_state.shape, f32),
         ((T, R, W), bf16),
         ((N, J, R, W), bf16),
         ((N, J, R, W), bf16),
@@ -379,24 +400,23 @@
     ]
     updated, next_state = pl.pallas_call(
         functools.partial(kernel, c),
-        out_shape=(jax.ShapeDtypeStruct((R, W), bf16), jax.ShapeDtypeStruct(ret_state.shape, f32)),
-        in_specs=[V] * 11 + [A] * 9,
-        out_specs=(V, A),
+        out_shape=(pltpu.VMEM((R, W), bf16), pltpu.VMEM(ret_state.shape, f32)),
+        in_specs=[A] * 20,
+        out_specs=(V, V),
         scratch_shapes=[pltpu.VMEM(shape, kind) for shape, kind in names] + [
             pltpu.SemaphoreType.DMA((4, T)),
             pltpu.SemaphoreType.DMA((4, T)),
             pltpu.SemaphoreType.DMA((4, N)),
             pltpu.SemaphoreType.DMA((4, N)),
-            pltpu.SemaphoreType.DMA((7 + 2 * local_experts,)),
-            pltpu.SemaphoreType.DMA,
+            pltpu.SemaphoreType.DMA((18 + 2 * local_experts,)),
         ],
         compiler_params=pltpu.CompilerParams(
-            collective_id=0, has_side_effects=True, vmem_limit_bytes=48 * 1024 * 1024
+            collective_id=0, has_side_effects=True, vmem_limit_bytes=56 * 1024 * 1024
         ),
-    )(hidden, positions.reshape(R, 1), jnp.asarray(inv), head_gain.reshape(1, HW), mix_gain.reshape(1, D),
-      ffn_gain.reshape(1, D), route_ids, route_weight, jnp.asarray(tab), jnp.asarray(perm, bf16),
+    )(*(pltpu.with_memory_space_constraint(x, pltpu.HBM) for x in (hidden, positions.reshape(1, R), jnp.asarray(inv), head_gain.reshape(1, HW), mix_gain.reshape(1, D),
+      ffn_gain.reshape(1, D), route_ids.T, route_weight.T, jnp.asarray(tab), jnp.asarray(perm, bf16),
       jnp.asarray(perm.T, bf16),
-      query_weight, key_weight, value_weight, gate_weight, out_weight, expert_gate, expert_up, expert_down, ret_state)
+      query_weight, key_weight, value_weight, gate_weight, out_weight, expert_gate, expert_up, expert_down, ret_state)))
     return updated, next_state
 
 

time: 75.7 us -> 58.1 us (0.77)
  local copies, waits for them, and re-layouts: 19.8 us -> 2.98 us
    unnamed x30 -> x2, local copies, waits for them, and re-layouts: 19 us -> 2.98 us
where the time goes in v2:
time: 58.1 us; the launch traced here: 57.9 us
  Pallas kernels  54.3 us (93%)
  local copies, waits for them, and re-layouts  2.98 us (5%)
  between operations  0.65 us (1%)
    pallas_call x1, Pallas kernels, per_device(): pl.pallas_call(functools.partial(kernel, c), out_shape=(pltpu.VMEM((R, W)...  54.3 us
    unnamed x2, local copies, waits for them, and re-layouts  2.98 us

profile of v2, /device:TPU:0, one launch (start us, length us, event | category | flops | bytes accessed | tf_op | source)
XLA Modules:
  0.0 57.9 jit_solution(14550669842288688024)
XLA Ops:
  0.6 54.3 %shard_map.203 = (bf16[40,512]{1,0:T(8,128)(2,1)S(1)}, f32[40,2,128,128]{3,2,1,0:T(8,128)S(1)}) custom-call(bf16[40,512]{1,0:T(8,128)(2,1)} %hid_h.1, s32[1,40]{1,0:T(1,128)} %bitcast.11, f32[1,128]{1,0:T(1,128)} %constant.8.clone.inv_h, f32[1,256]{1,0:T(1,128)} %bitcast.8, f32[1,4096]{1,0:T(1,128)} %bitcast.6, f32[1,4096]{1,0:T(1,128)} %bitcast.7, ...), custom_call_target="tpu_custom_call" | custom-call | tf_op jit(solution)/shard_map/pallas_call | solution.py:401
  55.0 0.6 %copy.24 = bf16[40,512]{1,0:T(8,128)(2,1)} copy(bf16[40,512]{1,0:T(8,128)(2,1)S(1)} %get-tuple-element.2) | data formatting | bytes 81920
  55.6 2.4 %copy.25 = f32[40,2,128,128]{3,2,1,0:T(8,128)} copy(f32[40,2,128,128]{3,2,1,0:T(8,128)S(1)} %get-tuple-element.3) | data formatting | bytes 10485760
